TPU v7x, 32 devices: a whole 2x2x4 slice. The times are simulated.
32 devices in a mesh: grp: 2 (over y), ep: 16 (over z, x, core), tp: 1.
Axes of the slice: x: 2, y: 2, z: 4, core: 2. Of those that a mesh axis runs over, the one named last changes fastest.
Arguments:
- tokens: bfloat16 [2048, 2048], P(('grp', 'ep')), parts along dimension 0, may hold values from -6 to 6
- norm_gain: float32 [2048], replicated, may hold values from 0.1 to 1.9
- routes: int32 [2048, 6], P(('grp', 'ep')), parts along dimension 0, may hold values from 0 to 15, all different within a row; in each aligned block of 64 rows (0 to 63, 64 to 127, ...) at most 48 rows name the same one
- route_weights: float32 [2048, 6], P(('grp', 'ep')), parts along dimension 0, may hold values from 0.05 to 1
- w_gate: bfloat16 [16, 2048, 2048], P('ep', None, 'tp'), may hold values from -0.125 to 0.125
- w_up: bfloat16 [16, 2048, 2048], P('ep', None, 'tp'), may hold values from -0.125 to 0.125
- w_down: bfloat16 [16, 2048, 2048], P('ep', 'tp'), may hold values from -4 to 4
- final_gain: float32 [2048], P('tp'), may hold values from 0.1 to 1.9
Outputs:
- mixed_out: bfloat16 [2048, 2048], P(('grp', 'ep'), 'tp'), parts along dimension 0
There are 2 independent parts, one for each index of `grp`. A program takes and returns all parts, laid end to end along the dimension named above; an argument that names none is the same for every part. Nothing has to cross between parts.
Inputs may be any that keep to these rules, and one draw needn't show every extreme that they name: `routes`: each row names 6 different experts; within the rows of one index of ep no expert is named by more than 48 rows, and in every draw some expert is named by exactly 48 rows of some index.
All inputs are finite; a program needn't handle non-finite values.
Results may differ from a plain program's by a relative error of at most 0.015.
Values may be sent and summed in bfloat16 or wider, within the bound.
No kernel may reach another device: no remote copies, remote signals or barrier semaphores. Data moves between devices by JAX's collectives and lax.ppermute only.
A program may use at most 64 MiB of HBM per device.

v0:
```python
import jax
import jax.numpy as jnp
from jax import lax
from jax.sharding import PartitionSpec as P

TOP_K = 6
EPS = 1e-06


def slot_table(route_rows, experts_all, capacity):
    flattened = route_rows.reshape(-1)
    matches = (flattened[:, None] == jnp.arange(experts_all, dtype=jnp.int32)[None, :]).astype(
        jnp.int32
    )
    earlier = jnp.cumsum(matches, axis=0) - matches
    slot_of = jnp.sum(earlier * matches, axis=1)
    return (flattened * capacity + slot_of).reshape(route_rows.shape)


def per_device(tokens, norm_gain, routes, route_weights, w_gate, w_up, w_down, final_gain):
    tok_count, features = tokens.shape
    ep_size = lax.axis_size("ep")
    exp_local = w_gate.shape[0]
    experts_all = exp_local * ep_size
    capacity = max(2, min(tok_count, 2 * tok_count * TOP_K // experts_all))
    slot_count = experts_all * capacity
    tokens_f = tokens.astype(jnp.float32)
    inverse = lax.rsqrt(jnp.mean(tokens_f * tokens_f, axis=1, keepdims=True) + EPS)
    normed = (tokens_f * inverse * norm_gain[None, :]).astype(jnp.bfloat16)
    places = slot_table(routes, experts_all, capacity)
    slot_ids = jnp.arange(slot_count, dtype=jnp.int32)
    matched = places[:, :, None] == slot_ids[None, None, :]
    selector = jnp.sum(matched.astype(jnp.float32), axis=1).T.astype(jnp.bfloat16)
    combine_rows = jnp.sum(jnp.where(matched, route_weights[:, :, None], 0.0), axis=1)
    outgoing = jnp.dot(selector, normed, preferred_element_type=jnp.float32).astype(jnp.bfloat16)
    outgoing = outgoing.reshape(ep_size, exp_local, capacity, features)
    received = lax.all_to_all(outgoing, "ep", split_axis=0, concat_axis=0, tiled=True)
    gate_value = jnp.einsum("secd,edf->secf", received, w_gate, preferred_element_type=jnp.float32)
    up_value = jnp.einsum("secd,edf->secf", received, w_up, preferred_element_type=jnp.float32)
    hidden = (jax.nn.silu(gate_value) * up_value).astype(jnp.bfloat16)
    partial_value = jnp.einsum("secf,efd->secd", hidden, w_down, preferred_element_type=jnp.float32)
    summed = lax.psum_scatter(
        partial_value.astype(jnp.bfloat16), "tp", scatter_dimension=3, tiled=True
    )
    returned = lax.all_to_all(summed, "ep", split_axis=0, concat_axis=0, tiled=True)
    results = returned.reshape(slot_count, returned.shape[3]).astype(jnp.float32)
    combined = jnp.dot(combine_rows, results, precision=lax.Precision.HIGHEST)
    local_squares = jnp.sum(combined * combined, axis=1)
    squares_all = lax.psum(local_squares, "tp")
    inverse_out = lax.rsqrt(squares_all / features + EPS)
    return (combined * inverse_out[:, None] * final_gain[None, :]).astype(jnp.bfloat16)


def solution(mesh):
    placed = (
        P(("grp", "ep"), None),
        P(),
        P(("grp", "ep"), None),
        P(("grp", "ep"), None),
        P("ep", None, "tp"),
        P("ep", None, "tp"),
        P("ep", "tp", None),
        P("tp"),
    )
    return jax.shard_map(
        per_device, mesh=mesh, in_specs=placed, out_specs=P(("grp", "ep"), "tp"), check_vma=False
    )
```

profile of v0, /device:TPU:1, one launch (start us, length us, event | category | flops | bytes accessed | tf_op | source)
XLA Modules:
  0.0 194.4 jit_solution(3700836418852448338)
XLA Ops:
  0.0 0.8 copy.33
  0.8 0.1 eq.42
  0.9 0.1 eq.38
  1.1 1.1 fusion.33
  2.2 0.9 reduce-window.6
  3.1 0.2 slice_reduce_fusion
  3.3 0.1 fusion.42
  3.4 0.1 reduce_sum.48
  3.6 0.1 copy.36
  3.6 0.0 copy-start.1
  3.6 0.9 multiply_add_fusion
  4.5 1.1 convert_reduce_fusion
  5.6 2.4 %convolution_convert_fusion = bf16[768,2048]{1,0:T(8,128)(2,1)S(1)} fusion(bf16[64,2048]{1,0:T(8,128)(2,1)} %param.8, f32[2048]{0:T(1024)} %param.9, f32[64]{0:T(128)S(1)} %add_rsqrt_fusion.1, bf16[64,768]{1,0:T(8,128)(2,1)S(1)} %get-tuple-element.5), kind=kOutput, calls=%fused_computation.14 | convolution fusion | flops 203423744 | bytes 3514624 | tf_op jit(solution)/shard_map/dot_general | solution.py:35
  8.0 77.3 %all_to_all.10 = bf16[16,1,48,2048]{3,2,1,0:T(8,128)(2,1)S(1)} all-to-all(bf16[16,1,48,2048]{3,2,1,0:T(8,128)(2,1)S(1)} %bitcast.110), channel_id=1, replica_groups=mesh['grp'=2,'ep'=16,'tp'=1] {'ep'}, dimensions={0} | all-to-all | bytes 6291456 | tf_op jit(solution)/shard_map/all_to_all | solution.py:37
  85.3 0.0 copy-done.1
  85.3 8.6 %fusion.4 = f32[16,48,2048]{2,1,0:T(8,128)} fusion(bf16[1,2048,2048]{2,1,0:T(8,128)(2,1)S(1)} %copy-done.1, bf16[16,1,48,2048]{3,2,1,0:T(8,128)(2,1)S(1)} %all_to_all.10), kind=kOutput, calls=%fused_computation.4 | convolution fusion | flops 6442450944 | bytes 17825792 | tf_op jit(solution)/shard_map/secd,edf->secf/dot_general | solution.py:38
  93.8 22.9 %fusion.24 = bf16[16,1,48,2048]{3,2,1,0:T(8,128)(2,1)} fusion(bf16[1,2048,2048]{2,1,0:T(8,128)(2,1)} %param.14, bf16[1,2048,2048]{2,1,0:T(8,128)(2,1)} %param.13, f32[16,48,2048]{2,1,0:T(8,128)} %fusion.4, bf16[16,1,48,2048]{3,2,1,0:T(8,128)(2,1)S(1)} %all_to_all.10), kind=kOutput, calls=%fused_computation.19 | convolution fusion | flops 12895911936 | bytes 29360128 | tf_op jit(solution)/shard_map/secf,efd->secd/dot_general | solution.py:41
  116.7 0.0 copy-start
  116.7 75.0 %all_to_all.11 = bf16[16,1,48,2048]{3,2,1,0:T(8,128)(2,1)S(1)} all-to-all(bf16[16,1,48,2048]{3,2,1,0:T(8,128)(2,1)} %fusion.24), channel_id=1, replica_groups=mesh['grp'=2,'ep'=16,'tp'=1] {'ep'}, dimensions={0} | all-to-all | bytes 6291456 | tf_op jit(solution)/shard_map/all_to_all | solution.py:45
  191.7 1.9 multiply_reduce_fusion
  193.6 0.0 copy-done
  193.6 0.8 multiply_convert_fusion
  (4 shorter events, 0.1 us)
Async XLA Ops:
  3.6 81.7 %copy-start.1 = (bf16[1,2048,2048]{2,1,0:T(8,128)(2,1)S(1)}, bf16[1,2048,2048]{2,1,0:T(8,128)(2,1)}, u32[]{:S(2)}) copy-start(bf16[1,2048,2048]{2,1,0:T(8,128)(2,1)} %param.12) | copy-start | bytes 25165828
  116.7 76.9 %copy-start = (f32[2048]{0:T(1024)S(1)}, f32[2048]{0:T(1024)}, u32[]{:S(2)}) copy-start(f32[2048]{0:T(1024)} %param.15) | copy-start | bytes 24580
where the time goes:
time: 195 us; the launch traced here: 194 us
  blocking collectives  152 us (78%)
  matrix products  35.7 us (18%)
  other arithmetic  4.93 us (3%)
    all_to_all x1, blocking collectives, per_device(): lax.all_to_all(outgoing, 'ep', split_axis=0, concat_axis=0, tiled=True)  77.3 us
    all_to_all x1, blocking collectives, per_device(): lax.all_to_all(summed, 'ep', split_axis=0, concat_axis=0, tiled=True)  75 us
    dot_general x1, matrix products, per_device(): jnp.einsum('secf,efd->secd', hidden, w_down, preferred_element_type=jnp.f...  22.9 us
    dot_general x1, matrix products, per_device(): jnp.einsum('secd,edf->secf', received, w_gate, preferred_element_type=jnp...  8.55 us

commit v1 on v0

--- a/solution.py
+++ b/solution.py
@@ -5,6 +5,17 @@
 
 TOP_K = 6
 EPS = 1e-06
+
+
+def cut_along(value, dim, count):
+    before, after = (value.shape[:dim], value.shape[dim + 1 :])
+    return jnp.moveaxis(value.reshape(*before, count, -1, *after), dim, 0)
+
+
+def in_order(blocks, dim):
+    shape = list(blocks.shape[1:])
+    shape[dim] *= blocks.shape[0]
+    return jnp.moveaxis(blocks, 0, dim).reshape(shape)
 
 
 def slot_table(route_rows, experts_all, capacity):
@@ -42,7 +53,14 @@
     summed = lax.psum_scatter(
         partial_value.astype(jnp.bfloat16), "tp", scatter_dimension=3, tiled=True
     )
-    returned = lax.all_to_all(summed, "ep", split_axis=0, concat_axis=0, tiled=True)
+    length, index = (lax.axis_size("ep"), lax.axis_index("ep"))
+    parts = cut_along(summed, 0, length)
+    outs = [parts[index]]
+    for step in range(1, length):
+        sent = parts[index ^ step]
+        outs.append(lax.ppermute(sent, "ep", [(i, i ^ step) for i in range(length)]))
+    parts = jnp.stack(outs)[index ^ jnp.arange(length)]
+    returned = in_order(parts, 0)
     results = returned.reshape(slot_count, returned.shape[3]).astype(jnp.float32)
     combined = jnp.dot(combine_rows, results, precision=lax.Precision.HIGHEST)
     local_squares = jnp.sum(combined * combined, axis=1)

time: 195 us -> 211 us (1.082)
  the two profiles are of different devices: /device:TPU:1 before, /device:TPU:21 now
where the time goes in v1:
time: 211 us; the launch traced here: 210 us
  waiting for transfers between devices  117 us (55%)
  starting transfers between devices  40.6 us (19%)
  matrix products  39 us (18%)
  local copies, waits for them, and re-layouts  9 us (4%)
  other arithmetic  4.66 us (2%)
    all_to_all x1, waiting for transfers between devices, per_device(): lax.all_to_all(outgoing, 'ep', split_axis=0, concat_axis=0, tiled=True)  69.5 us
    ppermute x15, waiting for transfers between devices, per_device(): lax.ppermute(sent, 'ep', [(i, i ^ step) for i in range(length)])  47.3 us
    ppermute x15, starting transfers between devices, per_device(): lax.ppermute(sent, 'ep', [(i, i ^ step) for i in range(length)])  34.2 us
    dot_general x1, matrix products, per_device(): jnp.einsum('secf,efd->secd', hidden, w_down, preferred_element_type=jnp.f...  22.9 us
    dot_general x1, matrix products, per_device(): jnp.einsum('secd,edf->secf', received, w_gate, preferred_element_type=jnp...  10.7 us
    all_to_all x1, starting transfers between devices, per_device(): lax.all_to_all(outgoing, 'ep', split_axis=0, concat_axis=0, tiled=True)  6.43 us
  transfers between devices with their start and end apart: 16, of which 11 were waited for; matrix products, arithmetic and copies ran while one was open for 1% of the time, Pallas kernels for 0%

profile of v1, /device:TPU:21, one launch (start us, length us, event | category | flops | bytes accessed | tf_op | source)
XLA Modules:
  0.0 210.3 jit_solution(4417502161371064930)
XLA Ops:
  0.0 0.8 copy.31
  0.8 0.1 eq.38
  0.9 0.1 eq.42
  1.1 0.9 reduce-window.6
  1.9 0.2 slice_reduce_fusion
  2.2 0.1 fusion.33
  2.3 0.1 reduce_sum.48
  2.4 0.1 copy.34
  2.5 0.7 multiply_add_fusion
  3.2 1.1 fusion.24
  4.3 1.0 convert_reduce_fusion
  5.3 3.7 %convolution_convert_fusion = bf16[768,2048]{1,0:T(8,128)(2,1)} fusion(bf16[64,2048]{1,0:T(8,128)(2,1)} %param.8, f32[2048]{0:T(1024)} %param.9, f32[64]{0:T(128)S(1)} %add_rsqrt_fusion.1, bf16[64,768]{1,0:T(8,128)(2,1)S(1)} %get-tuple-element.5), kind=kOutput, calls=%fused_computation.15 | convolution fusion | flops 203423744 | bytes 3514624 | tf_op jit(solution)/shard_map/dot_general | solution.py:46
  9.0 6.4 %all-to-all-start = ((bf16[16,1,48,2048]{3,2,1,0:T(8,128)(2,1)}), bf16[16,1,48,2048]{3,2,1,0:T(8,128)(2,1)S(1)}, u32[]{:S(2)}, u32[]{:S(2)}) async-start(bf16[16,1,48,2048]{3,2,1,0:T(8,128)(2,1)} %bitcast.2), calls=%async_computation | async-start | bytes 6291456 | tf_op jit(solution)/shard_map/all_to_all | solution.py:48
  15.5 69.5 %all-to-all-done = bf16[16,1,48,2048]{3,2,1,0:T(8,128)(2,1)S(1)} async-done(((bf16[16,1,48,2048]{3,2,1,0:T(8,128)(2,1)}), bf16[16,1,48,2048]{3,2,1,0:T(8,128)(2,1)S(1)}, u32[]{:S(2)}, u32[]{:S(2)}) %all-to-all-start) | async-done | bytes 3145760 | tf_op jit(solution)/shard_map/all_to_all | solution.py:48
  84.9 10.7 %fusion.4 = f32[16,48,2048]{2,1,0:T(8,128)} fusion(bf16[1,2048,2048]{2,1,0:T(8,128)(2,1)} %param.12, bf16[16,1,48,2048]{3,2,1,0:T(8,128)(2,1)S(1)} %all-to-all-done), kind=kOutput, calls=%fused_computation.5 | convolution fusion | flops 6442450944 | bytes 17825792 | tf_op jit(solution)/shard_map/secd,edf->secf/dot_general | solution.py:49
  95.6 22.9 %fusion.12 = bf16[16,48,2048]{2,1,0:T(8,128)(2,1)} fusion(bf16[1,2048,2048]{2,1,0:T(8,128)(2,1)} %param.14, f32[16,48,2048]{2,1,0:T(8,128)} %fusion.4, bf16[1,2048,2048]{2,1,0:T(8,128)(2,1)} %param.13, bf16[16,1,48,2048]{3,2,1,0:T(8,128)(2,1)S(1)} %all-to-all-done), kind=kOutput, calls=%fused_computation.14 | convolution fusion | flops 12895911936 | bytes 29360128 | tf_op jit(solution)/shard_map/secf,efd->secd/dot_general | solution.py:52
  118.5 2.1 dynamic-slice_bitcast_fusion
  120.6 1.0 collective-permute-start
  121.6 0.0 collective-permute-start.1
  121.6 1.7 collective-permute-start.2
  123.3 0.0 collective-permute-start.3
  123.3 1.8 collective-permute-start.4
  125.1 0.9 bitcast_dynamic-update-slice_fusion
  126.0 0.7 collective-permute-start.5
  126.8 1.2 collective-permute-done.1
  128.0 2.3 %collective-permute-start.6 = (bf16[1,1,48,2048]{3,2,1,0:T(8,128)(2,1)S(1)}, bf16[1,1,48,2048]{3,2,1,0:T(8,128)(2,1)S(1)}, u32[]{:S(2)}, u32[]{:S(2)}) collective-permute-start(bf16[1,1,48,2048]{3,2,1,0:T(8,128)(2,1)S(1)} %get-tuple-element.15), channel_id=1, source_target_pairs={{0,7},{1,6},{2,5},{3,4},{4,3},{5,2},{6,1},{7,0},{8,15},{9,14},{10,... | collective-permute-start | bytes 589832 | tf_op jit(solution)/shard_map/ppermute | solution.py:61
  130.3 2.4 %collective-permute-done.2 = bf16[1,1,48,2048]{3,2,1,0:T(8,128)(2,1)S(1)} collective-permute-done((bf16[1,1,48,2048]{3,2,1,0:T(8,128)(2,1)S(1)}, bf16[1,1,48,2048]{3,2,1,0:T(8,128)(2,1)S(1)}, u32[]{:S(2)}, u32[]{:S(2)}) %collective-permute-start.2) | collective-permute-done | bytes 196640 | tf_op jit(solution)/shard_map/ppermute | solution.py:61
  132.7 0.0 collective-permute-start.7
  132.8 0.0 collective-permute-done.3
  132.8 2.4 %collective-permute-start.8 = (bf16[1,1,48,2048]{3,2,1,0:T(8,128)(2,1)S(1)}, bf16[1,1,48,2048]{3,2,1,0:T(8,128)(2,1)S(1)}, u32[]{:S(2)}, u32[]{:S(2)}) collective-permute-start(bf16[1,1,48,2048]{3,2,1,0:T(8,128)(2,1)S(1)} %get-tuple-element.13), channel_id=1, source_target_pairs={{0,9},{1,8},{2,11},{3,10},{4,13},{5,12},{6,15},{7,14},{8,1},{9,0},... | collective-permute-start | bytes 589832 | tf_op jit(solution)/shard_map/ppermute | solution.py:61
  135.2 0.1 collective-permute-start.9
  135.3 8.3 %collective-permute-done.5 = bf16[1,1,48,2048]{3,2,1,0:T(8,128)(2,1)S(1)} collective-permute-done((bf16[1,1,48,2048]{3,2,1,0:T(8,128)(2,1)S(1)}, bf16[1,1,48,2048]{3,2,1,0:T(8,128)(2,1)S(1)}, u32[]{:S(2)}, u32[]{:S(2)}) %collective-permute-start.5) | collective-permute-done | bytes 196640 | tf_op jit(solution)/shard_map/ppermute | solution.py:61
  143.7 4.7 %collective-permute-start.10 = (bf16[1,1,48,2048]{3,2,1,0:T(8,128)(2,1)S(1)}, bf16[1,1,48,2048]{3,2,1,0:T(8,128)(2,1)S(1)}, u32[]{:S(2)}, u32[]{:S(2)}) collective-permute-start(bf16[1,1,48,2048]{3,2,1,0:T(8,128)(2,1)S(1)} %get-tuple-element.11), channel_id=1, source_target_pairs={{0,11},{1,10},{2,9},{3,8},{4,15},{5,14},{6,13},{7,12},{8,3},{9,2},... | collective-permute-start | bytes 589832 | tf_op jit(solution)/shard_map/ppermute | solution.py:61
  148.4 0.7 collective-permute-start.11
  149.1 1.3 collective-permute-start.12
  150.4 0.9 collective-permute-done.8
  151.2 17.4 %collective-permute-start.13 = (bf16[1,1,48,2048]{3,2,1,0:T(8,128)(2,1)S(1)}, bf16[1,1,48,2048]{3,2,1,0:T(8,128)(2,1)S(1)}, u32[]{:S(2)}, u32[]{:S(2)}) collective-permute-start(bf16[1,1,48,2048]{3,2,1,0:T(8,128)(2,1)S(1)} %get-tuple-element.8), channel_id=1, source_target_pairs={{0,14},{1,15},{2,12},{3,13},{4,10},{5,11},{6,8},{7,9},{8,6},{9,7},... | collective-permute-start | bytes 589832 | tf_op jit(solution)/shard_map/ppermute | solution.py:61
  168.7 6.7 %collective-permute-done.9 = bf16[1,1,48,2048]{3,2,1,0:T(8,128)(2,1)S(1)} collective-permute-done((bf16[1,1,48,2048]{3,2,1,0:T(8,128)(2,1)S(1)}, bf16[1,1,48,2048]{3,2,1,0:T(8,128)(2,1)S(1)}, u32[]{:S(2)}, u32[]{:S(2)}) %collective-permute-start.9) | collective-permute-done | bytes 196640 | tf_op jit(solution)/shard_map/ppermute | solution.py:61
  175.4 4.2 %collective-permute-done.10 = bf16[1,1,48,2048]{3,2,1,0:T(8,128)(2,1)S(1)} collective-permute-done((bf16[1,1,48,2048]{3,2,1,0:T(8,128)(2,1)S(1)}, bf16[1,1,48,2048]{3,2,1,0:T(8,128)(2,1)S(1)}, u32[]{:S(2)}, u32[]{:S(2)}) %collective-permute-start.10) | collective-permute-done | bytes 196640 | tf_op jit(solution)/shard_map/ppermute | solution.py:61
  179.6 9.5 %collective-permute-done.11 = bf16[1,1,48,2048]{3,2,1,0:T(8,128)(2,1)S(1)} collective-permute-done((bf16[1,1,48,2048]{3,2,1,0:T(8,128)(2,1)S(1)}, bf16[1,1,48,2048]{3,2,1,0:T(8,128)(2,1)S(1)}, u32[]{:S(2)}, u32[]{:S(2)}) %collective-permute-start.11) | collective-permute-done | bytes 196640 | tf_op jit(solution)/shard_map/ppermute | solution.py:61
  189.2 4.5 %collective-permute-done.12 = bf16[1,1,48,2048]{3,2,1,0:T(8,128)(2,1)S(1)} collective-permute-done((bf16[1,1,48,2048]{3,2,1,0:T(8,128)(2,1)S(1)}, bf16[1,1,48,2048]{3,2,1,0:T(8,128)(2,1)S(1)}, u32[]{:S(2)}, u32[]{:S(2)}) %collective-permute-start.12) | collective-permute-done | bytes 196640 | tf_op jit(solution)/shard_map/ppermute | solution.py:61
  193.7 5.4 %collective-permute-done.13 = bf16[1,1,48,2048]{3,2,1,0:T(8,128)(2,1)S(1)} collective-permute-done((bf16[1,1,48,2048]{3,2,1,0:T(8,128)(2,1)S(1)}, bf16[1,1,48,2048]{3,2,1,0:T(8,128)(2,1)S(1)}, u32[]{:S(2)}, u32[]{:S(2)}) %collective-permute-start.13) | collective-permute-done | bytes 196640 | tf_op jit(solution)/shard_map/ppermute | solution.py:61
  199.1 4.2 %collective-permute-done.14 = bf16[1,1,48,2048]{3,2,0,1:T(8,128)(2,1)S(1)} collective-permute-done((bf16[1,1,48,2048]{3,2,0,1:T(8,128)(2,1)S(1)}, bf16[1,1,48,2048]{3,2,0,1:T(8,128)(2,1)S(1)}, u32[]{:S(2)}, u32[]{:S(2)}) %collective-permute-start.14) | collective-permute-done | bytes 196640 | tf_op jit(solution)/shard_map/ppermute | solution.py:61
  203.3 1.7 copy-done
  205.0 2.6 %gather_fusion = bf16[16,48,2048]{2,1,0:T(8,128)(2,1)S(1)} fusion(bf16[16,48,2048]{2,1,0:T(8,128)(2,1)} %bitcast.221, s32[1024]{0:T(1024)S(1)} %pad_clamp_fusion), kind=kCustom, calls=%fused_computation | custom fusion | bytes 6291520 | tf_op jit(solution)/shard_map/gather | solution.py:62
  207.6 0.0 copy-start.1
  207.6 1.9 multiply_reduce_fusion
  209.5 0.8 multiply_convert_fusion
  (28 shorter events, 0.3 us)
Async XLA Ops:
  9.0 75.9 %all-to-all-start = ((bf16[16,1,48,2048]{3,2,1,0:T(8,128)(2,1)}), bf16[16,1,48,2048]{3,2,1,0:T(8,128)(2,1)S(1)}, u32[]{:S(2)}, u32[]{:S(2)}) async-start(bf16[16,1,48,2048]{3,2,1,0:T(8,128)(2,1)} %bitcast.2), calls=%async_computation | async-start | bytes 6291456 | tf_op jit(solution)/shard_map/all_to_all | solution.py:48
  120.6 5.5 %collective-permute-start = (bf16[1,1,48,2048]{3,2,1,0:T(8,128)(2,1)S(1)}, bf16[1,1,48,2048]{3,2,1,0:T(8,128)(2,1)S(1)}, u32[]{:S(2)}, u32[]{:S(2)}) collective-permute-start(bf16[1,1,48,2048]{3,2,1,0:T(8,128)(2,1)S(1)} %get-tuple-element.21), channel_id=1, source_target_pairs={{0,1},{1,0},{2,3},{3,2},{4,5},{5,4},{6,7},{7,6},{8,9},{9,8},{10,11... | collective-permute-start | bytes 589832 | tf_op jit(solution)/shard_map/ppermute | solution.py:61
  121.6 6.4 %collective-permute-start.1 = (bf16[1,1,48,2048]{3,2,1,0:T(8,128)(2,1)S(1)}, bf16[1,1,48,2048]{3,2,1,0:T(8,128)(2,1)S(1)}, u32[]{:S(2)}, u32[]{:S(2)}) collective-permute-start(bf16[1,1,48,2048]{3,2,1,0:T(8,128)(2,1)S(1)} %get-tuple-element.20), channel_id=1, source_target_pairs={{0,2},{1,3},{2,0},{3,1},{4,6},{5,7},{6,4},{7,5},{8,10},{9,11},{10,... | collective-permute-start | bytes 589832 | tf_op jit(solution)/shard_map/ppermute | solution.py:61
  121.6 11.1 %collective-permute-start.2 = (bf16[1,1,48,2048]{3,2,1,0:T(8,128)(2,1)S(1)}, bf16[1,1,48,2048]{3,2,1,0:T(8,128)(2,1)S(1)}, u32[]{:S(2)}, u32[]{:S(2)}) collective-permute-start(bf16[1,1,48,2048]{3,2,1,0:T(8,128)(2,1)S(1)} %get-tuple-element.19), channel_id=1, source_target_pairs={{0,3},{1,2},{2,1},{3,0},{4,7},{5,6},{6,5},{7,4},{8,11},{9,10},{10,... | collective-permute-start | bytes 589832 | tf_op jit(solution)/shard_map/ppermute | solution.py:61
  123.3 9.4 %collective-permute-start.3 = (bf16[1,1,48,2048]{3,2,1,0:T(8,128)(2,1)S(1)}, bf16[1,1,48,2048]{3,2,1,0:T(8,128)(2,1)S(1)}, u32[]{:S(2)}, u32[]{:S(2)}) collective-permute-start(bf16[1,1,48,2048]{3,2,1,0:T(8,128)(2,1)S(1)} %get-tuple-element.18), channel_id=1, source_target_pairs={{0,4},{1,5},{2,6},{3,7},{4,0},{5,1},{6,2},{7,3},{8,12},{9,13},{10,... | collective-permute-start | bytes 589832 | tf_op jit(solution)/shard_map/ppermute | solution.py:61
  123.3 11.9 %collective-permute-start.4 = (bf16[1,1,48,2048]{3,2,1,0:T(8,128)(2,1)S(1)}, bf16[1,1,48,2048]{3,2,1,0:T(8,128)(2,1)S(1)}, u32[]{:S(2)}, u32[]{:S(2)}) collective-permute-start(bf16[1,1,48,2048]{3,2,1,0:T(8,128)(2,1)S(1)} %get-tuple-element.17), channel_id=1, source_target_pairs={{0,5},{1,4},{2,7},{3,6},{4,1},{5,0},{6,3},{7,2},{8,13},{9,12},{10,... | collective-permute-start | bytes 589832 | tf_op jit(solution)/shard_map/ppermute | solution.py:61
  126.0 17.6 %collective-permute-start.5 = (bf16[1,1,48,2048]{3,2,1,0:T(8,128)(2,1)S(1)}, bf16[1,1,48,2048]{3,2,1,0:T(8,128)(2,1)S(1)}, u32[]{:S(2)}, u32[]{:S(2)}) collective-permute-start(bf16[1,1,48,2048]{3,2,1,0:T(8,128)(2,1)S(1)} %get-tuple-element.16), channel_id=1, source_target_pairs={{0,6},{1,7},{2,4},{3,5},{4,2},{5,3},{6,0},{7,1},{8,14},{9,15},{10,... | collective-permute-start | bytes 589832 | tf_op jit(solution)/shard_map/ppermute | solution.py:61
  128.0 20.4 %collective-permute-start.6 = (bf16[1,1,48,2048]{3,2,1,0:T(8,128)(2,1)S(1)}, bf16[1,1,48,2048]{3,2,1,0:T(8,128)(2,1)S(1)}, u32[]{:S(2)}, u32[]{:S(2)}) collective-permute-start(bf16[1,1,48,2048]{3,2,1,0:T(8,128)(2,1)S(1)} %get-tuple-element.15), channel_id=1, source_target_pairs={{0,7},{1,6},{2,5},{3,4},{4,3},{5,2},{6,1},{7,0},{8,15},{9,14},{10,... | collective-permute-start | bytes 589832 | tf_op jit(solution)/shard_map/ppermute | solution.py:61
  132.7 16.3 %collective-permute-start.7 = (bf16[1,1,48,2048]{3,2,1,0:T(8,128)(2,1)S(1)}, bf16[1,1,48,2048]{3,2,1,0:T(8,128)(2,1)S(1)}, u32[]{:S(2)}, u32[]{:S(2)}) collective-permute-start(bf16[1,1,48,2048]{3,2,1,0:T(8,128)(2,1)S(1)} %get-tuple-element.14), channel_id=1, source_target_pairs={{0,8},{1,9},{2,10},{3,11},{4,12},{5,13},{6,14},{7,15},{8,0},{9,1},... | collective-permute-start | bytes 589832 | tf_op jit(solution)/shard_map/ppermute | solution.py:61
  132.8 18.5 %collective-permute-start.8 = (bf16[1,1,48,2048]{3,2,1,0:T(8,128)(2,1)S(1)}, bf16[1,1,48,2048]{3,2,1,0:T(8,128)(2,1)S(1)}, u32[]{:S(2)}, u32[]{:S(2)}) collective-permute-start(bf16[1,1,48,2048]{3,2,1,0:T(8,128)(2,1)S(1)} %get-tuple-element.13), channel_id=1, source_target_pairs={{0,9},{1,8},{2,11},{3,10},{4,13},{5,12},{6,15},{7,14},{8,1},{9,0},... | collective-permute-start | bytes 589832 | tf_op jit(solution)/shard_map/ppermute | solution.py:61
  135.2 40.2 %collective-permute-start.9 = (bf16[1,1,48,2048]{3,2,1,0:T(8,128)(2,1)S(1)}, bf16[1,1,48,2048]{3,2,1,0:T(8,128)(2,1)S(1)}, u32[]{:S(2)}, u32[]{:S(2)}) collective-permute-start(bf16[1,1,48,2048]{3,2,1,0:T(8,128)(2,1)S(1)} %get-tuple-element.12), channel_id=1, source_target_pairs={{0,10},{1,11},{2,8},{3,9},{4,14},{5,15},{6,12},{7,13},{8,2},{9,3},... | collective-permute-start | bytes 589832 | tf_op jit(solution)/shard_map/ppermute | solution.py:61
  143.7 35.9 %collective-permute-start.10 = (bf16[1,1,48,2048]{3,2,1,0:T(8,128)(2,1)S(1)}, bf16[1,1,48,2048]{3,2,1,0:T(8,128)(2,1)S(1)}, u32[]{:S(2)}, u32[]{:S(2)}) collective-permute-start(bf16[1,1,48,2048]{3,2,1,0:T(8,128)(2,1)S(1)} %get-tuple-element.11), channel_id=1, source_target_pairs={{0,11},{1,10},{2,9},{3,8},{4,15},{5,14},{6,13},{7,12},{8,3},{9,2},... | collective-permute-start | bytes 589832 | tf_op jit(solution)/shard_map/ppermute | solution.py:61
  148.4 40.8 %collective-permute-start.11 = (bf16[1,1,48,2048]{3,2,1,0:T(8,128)(2,1)S(1)}, bf16[1,1,48,2048]{3,2,1,0:T(8,128)(2,1)S(1)}, u32[]{:S(2)}, u32[]{:S(2)}) collective-permute-start(bf16[1,1,48,2048]{3,2,1,0:T(8,128)(2,1)S(1)} %get-tuple-element.10), channel_id=1, source_target_pairs={{0,12},{1,13},{2,14},{3,15},{4,8},{5,9},{6,10},{7,11},{8,4},{9,5},... | collective-permute-start | bytes 589832 | tf_op jit(solution)/shard_map/ppermute | solution.py:61
  149.1 44.6 %collective-permute-start.12 = (bf16[1,1,48,2048]{3,2,1,0:T(8,128)(2,1)S(1)}, bf16[1,1,48,2048]{3,2,1,0:T(8,128)(2,1)S(1)}, u32[]{:S(2)}, u32[]{:S(2)}) collective-permute-start(bf16[1,1,48,2048]{3,2,1,0:T(8,128)(2,1)S(1)} %get-tuple-element.9), channel_id=1, source_target_pairs={{0,13},{1,12},{2,15},{3,14},{4,9},{5,8},{6,11},{7,10},{8,5},{9,4},... | collective-permute-start | bytes 589832 | tf_op jit(solution)/shard_map/ppermute | solution.py:61
  151.2 47.8 %collective-permute-start.13 = (bf16[1,1,48,2048]{3,2,1,0:T(8,128)(2,1)S(1)}, bf16[1,1,48,2048]{3,2,1,0:T(8,128)(2,1)S(1)}, u32[]{:S(2)}, u32[]{:S(2)}) collective-permute-start(bf16[1,1,48,2048]{3,2,1,0:T(8,128)(2,1)S(1)} %get-tuple-element.8), channel_id=1, source_target_pairs={{0,14},{1,15},{2,12},{3,13},{4,10},{5,11},{6,8},{7,9},{8,6},{9,7},... | collective-permute-start | bytes 589832 | tf_op jit(solution)/shard_map/ppermute | solution.py:61
  175.4 27.9 %collective-permute-start.14 = (bf16[1,1,48,2048]{3,2,0,1:T(8,128)(2,1)S(1)}, bf16[1,1,48,2048]{3,2,0,1:T(8,128)(2,1)S(1)}, u32[]{:S(2)}, u32[]{:S(2)}) collective-permute-start(bf16[1,1,48,2048]{3,2,0,1:T(8,128)(2,1)S(1)} %get-tuple-element.7), channel_id=1, source_target_pairs={{0,15},{1,14},{2,13},{3,12},{4,11},{5,10},{6,9},{7,8},{8,7},{9,6},... | collective-permute-start | bytes 589832 | tf_op jit(solution)/shard_map/ppermute | solution.py:61
  203.3 1.7 copy-start
  207.6 1.9 copy-start.1
